TPU v7x, 32 devices: a whole 2x2x4 slice. The times are simulated.
32 devices in a mesh: tp: 8 (over z, x), dp: 4 (over y, core).
Axes of the slice: x: 2, y: 2, z: 4, core: 2. Of those that a mesh axis runs over, the one named last changes fastest.
Arguments:
- tokens: bfloat16 [128, 4096], P('tp', 'dp'), may hold values from -6 to 6
- query_weight: bfloat16 [2, 4096, 2048], P(None, 'dp', 'tp'), may hold values from -0.09375 to 0.09375
- key_weight: bfloat16 [2, 4096, 2048], P(None, 'dp', 'tp'), may hold values from -0.09375 to 0.09375
- value_weight: bfloat16 [2, 4096, 2048], P(None, 'dp', 'tp'), may hold values from -0.09375 to 0.09375
- outgate_weight: bfloat16 [2, 4096, 2048], P(None, 'dp', 'tp'), may hold values from -0.09375 to 0.09375
- igate_weight: bfloat16 [2, 4096, 16], replicated, may hold values from -0.09375 to 0.09375
- fgate_weight: bfloat16 [2, 4096, 16], replicated, may hold values from -0.09375 to 0.09375
- norm_gain: float32 [2, 4096], P(None, 'dp'), may hold values from 0.1 to 1.9
- head_gain: float32 [2, 2048], P(None, 'tp'), may hold values from 0.1 to 1.9
- proj_weight: bfloat16 [2, 2048, 4096], P(None, 'tp', 'dp'), may hold values from -0.125 to 0.125
- cell_state: float32 [2, 128, 16, 128, 128], P(None, 'dp', 'tp'), may hold values from -1.8 to 1.8
- normer_state: float32 [2, 128, 16, 128], P(None, 'dp', 'tp'), may hold values from -1.8 to 1.8
- stab_state: float32 [2, 128, 16], P(None, 'dp', 'tp'), may hold values from -4 to 4
Outputs:
- final_rows: bfloat16 [128, 4096], P('tp', 'dp')
- cell_out: float32 [2, 128, 16, 128, 128], P(None, 'dp', 'tp')
- normer_out: float32 [2, 128, 16, 128], P(None, 'dp', 'tp')
- stab_out: float32 [2, 128, 16], P(None, 'dp', 'tp')
All inputs are finite; a program needn't handle non-finite values.
Results may differ from a plain program's by a relative error of at most 0.012.
The roundings to bfloat16 on the way count: a program that leaves them out, or rounds other values in their place, can miss the bound.
Values may be sent and summed in bfloat16 or wider, within the bound.
A program may use at most 64 MiB of HBM per device.

v0:
```python
import functools
import math

import jax
import jax.numpy as jnp
from jax import lax
from jax.experimental import pallas as pl
from jax.experimental.pallas import tpu as pltpu
from jax.sharding import PartitionSpec as P

EPSILON = 1e-06
F32 = jnp.float32
BF16 = jnp.bfloat16
MESH = pl.DeviceIdType.MESH


def split_axis(size):
    inner = max(f for f in range(1, math.isqrt(size) + 1) if size % f == 0)
    return size // inner, inner


def row_block(index, rows):
    return pl.ds(pl.multiple_of(index * rows, rows), rows)


def gate_dot(scaled, weight):
    return lax.dot_general(
        scaled, weight, (((1,), (1,)), ((), ())), preferred_element_type=F32
    )


def step_kernel(
    ntp,
    ndp,
    tokens,
    wq,
    wk,
    wv,
    wo,
    wig,
    wfg,
    norm_gain,
    head_gain,
    proj,
    cell,
    normer,
    stab,
    final_out,
    cell_buf,
    normer_out,
    stab_out,
    w_buf,
    ig_buf,
    fg_buf,
    proj_buf,
    written_buf,
    key_buf,
    keep_buf,
    tok_sem,
    small_sem,
    gain_buf,
    head_buf,
    normer_buf,
    stab_buf,
    split_buf,
    current,
    partial,
    gates,
    pair_recv,
    pair_gate,
    pair_sum,
    pair_gsum,
    proj_recv,
    gate_recv,
    gated_all,
    out_part,
    out_stage,
    out_recv,
    load_sem,
    cell_sem,
    ag_send,
    ag_recv,
    pr_send,
    pr_recv,
    pg_send,
    pg_recv,
    rs_send,
    rs_recv,
    gt_send,
    gt_recv,
    gg_send,
    gg_recv,
    os_send,
    os_recv,
):
    blocks = wq.shape[0]
    width, inner = wq.shape[1], wq.shape[2]
    all_heads = wig.shape[1]
    seqs, heads, dh = cell.shape[1], cell.shape[2], cell.shape[3]
    rows = tokens.shape[0]
    t = lax.axis_index("tp")
    d = lax.axis_index("dp")
    outer, side = split_axis(ntp)
    z = t // side
    x = lax.rem(t, side)

    pair = 2 if ndp % 2 == 0 else 1
    ring = ndp // pair
    y = d // pair
    core = lax.rem(d, pair)

    tok_load = pltpu.make_async_copy(tokens, current.at[0, row_block(t, rows)], tok_sem)
    tok_load.start()
    small = [
        pltpu.make_async_copy(src, dst, small_sem.at[i])
        for i, (src, dst) in enumerate(
            (
                (norm_gain, gain_buf),
                (head_gain, head_buf),
                (normer, normer_buf),
                (stab, stab_buf),
            )
        )
    ]
    loads = []
    for b in range(blocks):
        for i, w in enumerate((wq, wk, wv, wo)):
            loads.append(pltpu.make_async_copy(w.at[b], w_buf.at[b, i], load_sem.at[b, i]))
        loads.append(
            pltpu.make_async_copy(
                wig.at[b, :, row_block(d, width)], ig_buf.at[b], load_sem.at[b, 4]
            )
        )
        loads.append(
            pltpu.make_async_copy(
                wfg.at[b, :, row_block(d, width)], fg_buf.at[b], load_sem.at[b, 5]
            )
        )
        loads.append(pltpu.make_async_copy(proj.at[b], proj_buf.at[b], load_sem.at[b, 6]))
    cell_loads = [
        pltpu.make_async_copy(cell.at[b], cell_buf.at[b], cell_sem.at[b]) for b in range(blocks)
    ]
    per_block = 7
    for b in range(blocks):
        for c in loads[b * per_block : (b + 1) * per_block]:
            c.start()
        cell_loads[b].start()
        if b == 0:
            for c in small:
                c.start()

    barrier = pltpu.get_barrier_semaphore()
    for k in range(1, ntp):
        pl.semaphore_signal(
            barrier, inc=1, device_id={"tp": lax.rem(t + k, ntp)}, device_id_type=MESH
        )
    for k in range(1, ndp):
        pl.semaphore_signal(
            barrier, inc=1, device_id={"dp": lax.rem(d + k, ndp)}, device_id_type=MESH
        )
    pl.semaphore_wait(barrier, ntp - 1 + ndp - 1)
    tok_load.wait()

    def split_cells(b):
        cell_loads[b].wait()

        def one(i, _):
            for h in range(heads):
                whole = cell_buf[b, i, h]
                high = whole.astype(BF16)
                here = row_block(i, dh)
                split_buf[h, here, 0:dh] = high
                split_buf[h, here, dh : 2 * dh] = (whole - high.astype(F32)).astype(BF16)
            return 0

        lax.fori_loop(0, seqs, one, 0)

    eight = math.gcd(seqs, 8)

    def update_cells(b):
        def one(c, _):
            here = row_block(c, eight)
            keep = keep_buf[here, :]
            for h in range(heads):
                lanes = slice(h * dh, (h + 1) * dh)
                across = jnp.transpose(written_buf[here, lanes])
                keys = key_buf[here, lanes]
                for j in range(eight):
                    cell_buf[b, c * eight + j, h] = (
                        keep[j : j + 1, h : h + 1] * cell_buf[b, c * eight + j, h]
                        + across[:, j : j + 1] * keys[j : j + 1, :]
                    )
            return 0

        lax.fori_loop(0, seqs // eight, one, 0)

    def gather(b):
        buf = current.at[b]
        own_src = buf.at[row_block(t, rows)]

        def send(src, block, slot, dest):
            copy = pltpu.make_async_remote_copy(
                src_ref=src,
                dst_ref=buf.at[row_block(block, rows)],
                send_sem=ag_send.at[b, slot],
                recv_sem=ag_recv.at[b, slot],
                device_id={"tp": dest},
                device_id_type=MESH,
            )
            copy.start()
            return copy

        first, second = [], []
        for k in range(1, outer):
            dest = lax.rem(z + k, outer) * side + x
            first.append(send(own_src, t, k - 1, dest))
        for j in range(1, side):
            dest = z * side + lax.rem(x + j, side)
            second.append(send(own_src, t, outer - 1 + (j - 1) * outer, dest))
        if b == 0:
            split_cells(0)
            for c in small:
                c.wait()
        for k in range(1, outer):
            first[k - 1].wait_recv()
            block = lax.rem(z - k + outer, outer) * side + x
            for j in range(1, side):
                dest = z * side + lax.rem(x + j, side)
                second.append(
                    send(
                        buf.at[row_block(block, rows)],
                        block,
                        outer - 1 + (j - 1) * outer + k,
                        dest,
                    )
                )
        for c in second:
            c.wait_recv()
        for c in first + second:
            c.wait_send()

    for b in range(blocks):
        gather(b)
        for c in loads[b * per_block : (b + 1) * per_block]:
            c.wait()
        as_float = current[b].astype(F32)
        scaled = (as_float * gain_buf[b : b + 1, :]).astype(BF16)
        gates[b, :, 0:all_heads] = gate_dot(scaled, ig_buf[b])
        gates[b, :, all_heads : 2 * all_heads] = gate_dot(scaled, fg_buf[b])
        gates[b, :, 2 * all_heads : 2 * all_heads + 1] = jnp.sum(
            as_float * as_float, axis=1, keepdims=True
        )
        sends = []

        def send_rows(srcs, dsts, send_sems, recv_sems, slot, dest):
            started = []
            for src, dst, ss, rr in zip(srcs, dsts, send_sems, recv_sems):
                copy = pltpu.make_async_remote_copy(
                    src_ref=src,
                    dst_ref=dst,
                    send_sem=ss.at[b, slot],
                    recv_sem=rr.at[b, slot],
                    device_id={"dp": dest},
                    device_id_type=MESH,
                )
                copy.start()
                started.append(copy)
            sends.extend(started)
            return started

        for i in range(4):
            cols = slice(i * inner, (i + 1) * inner)
            partial[b, :, cols] = jnp.dot(scaled, w_buf[b, i], preferred_element_type=F32)
        paired = []
        if pair == 2:
            mate = y * pair + 1 - core
            for k in range(ring):
                slot = (k + 1) % ring
                block = row_block(lax.rem(y + slot, ring) * pair + 1 - core, seqs)
                paired.append(
                    (
                        slot,
                        send_rows(
                            (partial.at[b, block], gates.at[b, block]),
                            (pair_recv.at[b, slot], pair_gate.at[b, slot]),
                            (pr_send, pg_send),
                            (pr_recv, pg_recv),
                            slot,
                            mate,
                        ),
                    )
                )
        else:
            paired = [((k + 1) % ring, []) for k in range(ring)]
        arriving = []
        total = gate_sum = None
        for slot, copies in paired:
            for c in copies:
                c.wait_recv()
            dest = lax.rem(y + slot, ring) * pair + core
            block = row_block(dest, seqs)
            rows_sum, gsum = partial[b, block, :], gates[b, block, :]
            if copies:
                rows_sum = rows_sum + pair_recv[b, slot]
                gsum = gsum + pair_gate[b, slot]
            if slot == 0:
                total, gate_sum = rows_sum, gsum
            else:
                pair_sum[b, slot - 1] = rows_sum.astype(pair_sum.dtype)
                pair_gsum[b, slot - 1] = gsum
                arriving.append(
                    send_rows(
                        (pair_sum.at[b, slot - 1], pair_gsum.at[b, slot - 1]),
                        (proj_recv.at[b, slot - 1], gate_recv.at[b, slot - 1]),
                        (rs_send, gt_send),
                        (rs_recv, gt_recv),
                        slot - 1,
                        dest,
                    )
                )
        for k in range(ring - 1):
            for c in arriving[k]:
                c.wait_recv()
            total = total + proj_recv[b, k].astype(F32)
            gate_sum = gate_sum + gate_recv[b, k]
        own = row_block(d, seqs)
        inv_rms = lax.rsqrt(gate_sum[:, 2 * all_heads : 2 * all_heads + 1] / (width * ndp) + EPSILON)
        query = total[:, 0:inner] * inv_rms
        key = total[:, inner : 2 * inner] * inv_rms * (dh ** (-0.5))
        value = total[:, 2 * inner : 3 * inner] * inv_rms
        outgate = total[:, 3 * inner : 4 * inner] * inv_rms
        pre = gate_sum * inv_rms
        key_buf[...] = key
        wide = -(-2 * seqs // 128) * 128
        column = lax.broadcasted_iota(jnp.int32, (dh, wide), 1)
        reads = []
        for h in range(heads):
            lanes = slice(h * dh, (h + 1) * dh)
            high = query[:, lanes].astype(BF16)
            low = (query[:, lanes] - high.astype(F32)).astype(BF16)
            terms = [jnp.concatenate([a, a], 1) for a in (high, low)]
            if wide > 2 * seqs:
                terms.append(jnp.zeros((wide - 2 * seqs, 2 * dh), BF16))
            rhs = jnp.concatenate(terms, 0)
            acc = jnp.zeros((dh, wide), F32)
            for c in range(seqs // eight):
                prod = gate_dot(
                    split_buf[h, c * eight * dh : (c + 1) * eight * dh, :], rhs
                )
                for j in range(eight):
                    own_column = (column == c * eight + j) | (column == seqs + c * eight + j)
                    acc = jnp.where(own_column, prod[j * dh : (j + 1) * dh], acc)
            turned = jnp.transpose(acc)
            reads.append(turned[0:seqs] + turned[seqs : 2 * seqs])

        lane = lax.broadcasted_iota(jnp.int32, pre.shape, 1)
        aux = jnp.zeros(pre.shape, F32)
        for h in range(heads):
            lanes = slice(h * dh, (h + 1) * dh)
            head = t * heads + h
            igate = jnp.sum(jnp.where(lane == head, pre, 0.0), axis=1, keepdims=True)
            fpre = jnp.sum(jnp.where(lane == head + all_heads, pre, 0.0), axis=1, keepdims=True)
            lf = jnp.minimum(fpre, 0.0) - jnp.log1p(jnp.exp(-jnp.abs(fpre)))
            stab_row = jnp.broadcast_to(stab_buf[b, h : h + 1, :], (seqs, seqs))
            diag = lax.broadcasted_iota(jnp.int32, (seqs, seqs), 0) == (
                lax.broadcasted_iota(jnp.int32, (seqs, seqs), 1)
            )
            m0 = jnp.sum(jnp.where(diag, stab_row, 0.0), axis=1, keepdims=True)
            carried = lf + m0
            m1 = jnp.maximum(carried, igate)
            stab_out[b, h : h + 1, :] = jnp.sum(jnp.where(diag, m1, 0.0), axis=0, keepdims=True)
            keep = jnp.exp(carried - m1)
            write = jnp.exp(igate - m1)
            qh, kh = query[:, lanes], key[:, lanes]
            written = write * value[:, lanes]
            n1 = keep * normer_buf[b, :, h, :] + write * kh
            written_buf[:, lanes] = written
            normer_out[b, :, h, :] = n1
            aux = jnp.where(lane == h, keep, aux)
            numer = keep * reads[h] + written * jnp.sum(kh * qh, axis=1, keepdims=True)
            denom = jnp.maximum(jnp.abs(jnp.sum(n1 * qh, axis=1, keepdims=True)), 1.0)
            readout = numer / denom
            normed = readout * lax.rsqrt(
                jnp.mean(readout * readout, axis=1, keepdims=True) + EPSILON
            )
            normed = normed * head_buf[b : b + 1, lanes]
            gate = 1.0 / (1.0 + jnp.exp(-outgate[:, lanes]))
            gated_all[b, own, lanes] = (gate * normed).astype(BF16)
        keep_buf[...] = aux

        spread = []
        for k in range(1, ndp):
            copy = pltpu.make_async_remote_copy(
                src_ref=gated_all.at[b, own],
                dst_ref=gated_all.at[b, own],
                send_sem=gg_send.at[b, k - 1],
                recv_sem=gg_recv.at[b, k - 1],
                device_id={"dp": lax.rem(d + k, ndp)},
                device_id_type=MESH,
            )
            copy.start()
            spread.append(copy)
        for c in spread:
            c.wait_recv()
        part = jnp.dot(gated_all[b], proj_buf[b], preferred_element_type=F32)
        out_part[...] = part
        out_stage[b] = part.astype(BF16)
        outs = []
        for k in range(1, ntp):
            dest = lax.rem(t + k, ntp)
            copy = pltpu.make_async_remote_copy(
                src_ref=out_stage.at[b, row_block(dest, rows)],
                dst_ref=out_recv.at[b, k - 1],
                send_sem=os_send.at[b, k - 1],
                recv_sem=os_recv.at[b, k - 1],
                device_id={"tp": dest},
                device_id_type=MESH,
            )
            copy.start()
            outs.append(copy)
        update_cells(b)
        if b + 1 < blocks:
            split_cells(b + 1)
        for c in outs:
            c.wait_recv()
        summed = out_part[row_block(t, rows), :]
        for k in range(ntp - 1):
            summed = summed + out_recv[b, k].astype(F32)
        if b + 1 < blocks:
            current[b + 1, row_block(t, rows), :] = summed.astype(BF16)
        else:
            final_out[...] = summed.astype(BF16)
        for c in sends + spread + outs:
            c.wait_send()


def store_kernel(*refs):
    sems = refs[-1]
    half = (len(refs) - 1) // 2
    copies = [
        pltpu.make_async_copy(refs[i], refs[half + i], sems.at[i]) for i in range(half)
    ]
    for c in copies:
        c.start()
    for c in copies:
        c.wait()


def kernel_grant(*kept):
    return 67_043_328 - sum(a.size * a.dtype.itemsize for a in kept) - 65536


def per_device(ntp, ndp, *args):
    (tokens, wq, wk, wv, wo, wig, wfg, norm_gain, head_gain, proj, cell, normer, stab) = args
    blocks, width, inner = wq.shape
    all_heads = wig.shape[2]
    seqs, heads, dh = cell.shape[1], cell.shape[2], cell.shape[3]
    rows = tokens.shape[0]
    pair = 2 if ndp % 2 == 0 else 1
    ring = ndp // pair
    more = max(ring - 1, 1)
    wig, wfg, stab = (jnp.swapaxes(a, 1, 2) for a in (wig, wfg, stab))
    batch = rows * ntp
    lanes = -(-(2 * all_heads + 1) // 128) * 128
    vmem = pl.BlockSpec(memory_space=pltpu.VMEM)
    hbm = pl.BlockSpec(memory_space=pltpu.HBM)
    dma = pltpu.SemaphoreType.DMA
    results = pl.pallas_call(
        functools.partial(step_kernel, ntp, ndp),
        out_shape=(
            jax.ShapeDtypeStruct(tokens.shape, BF16),
            jax.ShapeDtypeStruct(cell.shape, F32),
            jax.ShapeDtypeStruct(normer.shape, F32),
            jax.ShapeDtypeStruct(stab.shape, F32),
        ),
        in_specs=[hbm] * 13,
        out_specs=(vmem,) * 4,
        scratch_shapes=[
            pltpu.VMEM((blocks, 4, width, inner), BF16),
            pltpu.VMEM((blocks, all_heads, width), BF16),
            pltpu.VMEM((blocks, all_heads, width), BF16),
            pltpu.VMEM(proj.shape, BF16),
            pltpu.VMEM((seqs, inner), F32),
            pltpu.VMEM((seqs, inner), F32),
            pltpu.VMEM((seqs, lanes), F32),
            dma,
            dma((4,)),
            pltpu.VMEM(norm_gain.shape, F32),
            pltpu.VMEM(head_gain.shape, F32),
            pltpu.VMEM(normer.shape, F32),
            pltpu.VMEM(stab.shape, F32),
            pltpu.VMEM((heads, seqs * dh, 2 * dh), BF16),
            pltpu.VMEM((blocks, batch, width), BF16),
            pltpu.VMEM((blocks, batch, 4 * inner), F32),
            pltpu.VMEM((blocks, batch, lanes), F32),
            pltpu.VMEM((blocks, ring, seqs, 4 * inner), F32),
            pltpu.VMEM((blocks, ring, seqs, lanes), F32),
            pltpu.VMEM((blocks, more, seqs, 4 * inner), F32),
            pltpu.VMEM((blocks, more, seqs, lanes), F32),
            pltpu.VMEM((blocks, more, seqs, 4 * inner), F32),
            pltpu.VMEM((blocks, more, seqs, lanes), F32),
            pltpu.VMEM((blocks, batch, inner), BF16),
            pltpu.VMEM((batch, width), F32),
            pltpu.VMEM((blocks, batch, width), BF16),
            pltpu.VMEM((blocks, ntp - 1, rows, width), BF16),
            dma((blocks, 7)),
            dma((blocks,)),
            dma((blocks, ntp - 1)),
            dma((blocks, ntp - 1)),
            dma((blocks, ring)),
            dma((blocks, ring)),
            dma((blocks, ring)),
            dma((blocks, ring)),
            dma((blocks, more)),
            dma((blocks, more)),
            dma((blocks, more)),
            dma((blocks, more)),
            dma((blocks, ndp - 1)),
            dma((blocks, ndp - 1)),
            dma((blocks, ntp - 1)),
            dma((blocks, ntp - 1)),
        ],
        compiler_params=pltpu.CompilerParams(
            collective_id=0, has_side_effects=True, vmem_limit_bytes=kernel_grant(cell, normer, tokens)
        ),
    )(tokens, wq, wk, wv, wo, wig, wfg, norm_gain, head_gain, proj, cell, normer, stab)

    shapes = tuple(jax.ShapeDtypeStruct(a.shape, a.dtype) for a in results)
    rows_out, cell_out, normer_out, stab_out = pl.pallas_call(
        store_kernel,
        out_shape=shapes,
        in_specs=[vmem] * 4,
        out_specs=(hbm,) * 4,
        scratch_shapes=[dma((4,))],
    )(*results)
    return rows_out, cell_out, normer_out, jnp.swapaxes(stab_out, 1, 2)


def solution(mesh):
    return jax.shard_map(
        functools.partial(per_device, mesh.shape["tp"], mesh.shape["dp"]),
        mesh=mesh,
        in_specs=(
            P("tp", "dp"),
            P(None, "dp", "tp"),
            P(None, "dp", "tp"),
            P(None, "dp", "tp"),
            P(None, "dp", "tp"),
            P(),
            P(),
            P(None, "dp"),
            P(None, "tp"),
            P(None, "tp", "dp"),
            P(None, "dp", "tp", None, None),
            P(None, "dp", "tp", None),
            P(None, "dp", "tp"),
        ),
        out_specs=(
            P("tp", "dp"),
            P(None, "dp", "tp", None, None),
            P(None, "dp", "tp", None),
            P(None, "dp", "tp"),
        ),
        check_vma=False,
    )
```

profile of v0, /device:TPU:0, one launch (start us, length us, event | category | flops | bytes accessed | tf_op | source)
XLA Modules:
  0.0 68.3 jit_solution(435649449838189762)
XLA Ops:
  0.6 60.8 %shard_map.156 = (bf16[16,1024]{1,0:T(8,128)(2,1)}, f32[2,32,2,128,128]{4,3,2,1,0:T(8,128)}, f32[2,32,2,128]{3,2,1,0:T(2,128)}, f32[2,2,32]{2,1,0:T(2,128)}) custom-call(bf16[16,1024]{1,0:T(8,128)(2,1)} %tokens.1, bf16[2,1024,256]{2,1,0:T(8,128)(2,1)} %wq.1, bf16[2,1024,256]{2,1,0:T(8,128)(2,1)} %wk.1, bf16[2,1024,256]{2,1,0:T(8,128)(2,1)} %wv.1, ...), custom_call_target="tpu_custom_call" | custom-call | tf_op jit(solution)/shard_map/pallas_call | solution.py:468
  61.4 6.8 %shard_map.157 = (bf16[16,1024]{1,0:T(8,128)(2,1)}, f32[2,32,2,128,128]{4,3,2,1,0:T(8,128)}, f32[2,32,2,128]{3,2,1,0:T(2,128)}, f32[2,2,32]{2,1,0:T(2,128)}) custom-call(bf16[16,1024]{1,0:T(8,128)(2,1)} %get-tuple-element.12.refs_0_, f32[2,32,2,128,128]{4,3,2,1,0:T(8,128)} %get-tuple-element.13.refs_1_, f32[2,32,2,128]{3,2,1,0:T(2,128)} %get-tuple-element.14.refs_2_, ...), custom_call_target="tpu_custom_call" | custom-call | tf_op jit(solution)/shard_map/pallas_call | solution.py:529
where the time goes:
time: 68.4 us; the launch traced here: 68.3 us
  Pallas kernels  67.6 us (99%)
    pallas_call x1, Pallas kernels, per_device(): pl.pallas_call(functools.partial(step_kernel, ntp, ndp), out_shape=(jax.S...  60.8 us
    pallas_call x1, Pallas kernels, per_device(): pl.pallas_call(store_kernel, out_shape=shapes, in_specs=[vmem] * 4, out_s...  6.83 us

commit v1 on v0

--- a/solution.py
+++ b/solution.py
@@ -434,20 +434,25 @@
             c.wait_send()
 
 
-def store_kernel(*refs):
-    sems = refs[-1]
-    half = (len(refs) - 1) // 2
+def store_kernel(rows, cell, normer, stab, rows_out, cell_out, normer_out, stab_out, cell_sem, sems):
+    blocks, seqs = cell.shape[0], cell.shape[1]
+    parts = cell_sem.shape[1]
+    step = seqs // parts
     copies = [
-        pltpu.make_async_copy(refs[i], refs[half + i], sems.at[i]) for i in range(half)
+        pltpu.make_async_copy(
+            cell.at[b, i * step : (i + 1) * step],
+            cell_out.at[b, i * step : (i + 1) * step],
+            cell_sem.at[b, i],
+        )
+        for b in range(blocks)
+        for i in range(parts)
     ]
+    for i, (src, dst) in enumerate(((rows, rows_out), (normer, normer_out), (stab, stab_out))):
+        copies.append(pltpu.make_async_copy(src, dst, sems.at[i]))
     for c in copies:
         c.start()
     for c in copies:
         c.wait()
-
-
-def kernel_grant(*kept):
-    return 67_043_328 - sum(a.size * a.dtype.itemsize for a in kept) - 65536
 
 
 def per_device(ntp, ndp, *args):
@@ -468,10 +473,10 @@
     results = pl.pallas_call(
         functools.partial(step_kernel, ntp, ndp),
         out_shape=(
-            jax.ShapeDtypeStruct(tokens.shape, BF16),
-            jax.ShapeDtypeStruct(cell.shape, F32),
-            jax.ShapeDtypeStruct(normer.shape, F32),
-            jax.ShapeDtypeStruct(stab.shape, F32),
+            pltpu.VMEM(tokens.shape, BF16),
+            pltpu.VMEM(cell.shape, F32),
+            pltpu.VMEM(normer.shape, F32),
+            pltpu.VMEM(stab.shape, F32),
         ),
         in_specs=[hbm] * 13,
         out_specs=(vmem,) * 4,
@@ -521,9 +526,16 @@
             dma((blocks, ntp - 1)),
         ],
         compiler_params=pltpu.CompilerParams(
-            collective_id=0, has_side_effects=True, vmem_limit_bytes=kernel_grant(cell, normer, tokens)
+            collective_id=0, has_side_effects=True, vmem_limit_bytes=40 << 20
         ),
-    )(tokens, wq, wk, wv, wo, wig, wfg, norm_gain, head_gain, proj, cell, normer, stab)
+    )(
+        *[
+            pltpu.with_memory_space_constraint(a, pltpu.HBM)
+            for a in (
+                tokens, wq, wk, wv, wo, wig, wfg, norm_gain, head_gain, proj, cell, normer, stab
+            )
+        ]
+    )
 
     shapes = tuple(jax.ShapeDtypeStruct(a.shape, a.dtype) for a in results)
     rows_out, cell_out, normer_out, stab_out = pl.pallas_call(
@@ -531,7 +543,8 @@
         out_shape=shapes,
         in_specs=[vmem] * 4,
         out_specs=(hbm,) * 4,
-        scratch_shapes=[dma((4,))],
+        scratch_shapes=[dma((blocks, math.gcd(seqs, 8))), dma((3,))],
+        compiler_params=pltpu.CompilerParams(vmem_limit_bytes=1 << 20),
     )(*results)
     return rows_out, cell_out, normer_out, jnp.swapaxes(stab_out, 1, 2)
 

time: 68.4 us -> 62 us (0.906)
  Pallas kernels: 67.6 us -> 61.2 us
    pallas_call x1, Pallas kernels: 6.83 us -> 3.48 us  [per_device(): pl.pallas_call(store_kernel, out_shape=shapes, in_specs=[vmem] * 4, out_s...]
    pallas_call x1, Pallas kernels: 60.8 us -> 57.7 us  [per_device(): pl.pallas_call(functools.partial(step_kernel, ntp, ndp), out_shape=(pltpu...]
where the time goes in v1:
time: 62 us; the launch traced here: 61.8 us
  Pallas kernels  61.2 us (99%)
  between operations  0.64 us (1%)
    pallas_call x1, Pallas kernels, per_device(): pl.pallas_call(functools.partial(step_kernel, ntp, ndp), out_shape=(pltpu...  57.7 us
    pallas_call x1, Pallas kernels, per_device(): pl.pallas_call(store_kernel, out_shape=shapes, in_specs=[vmem] * 4, out_s...  3.48 us

profile of v1, /device:TPU:0, one launch (start us, length us, event | category | flops | bytes accessed | tf_op | source)
XLA Modules:
  0.0 61.8 jit_solution(16246806702173192776)
XLA Ops:
  0.6 57.7 %shard_map.156 = (bf16[16,1024]{1,0:T(8,128)(2,1)S(1)}, f32[2,32,2,128,128]{4,3,2,1,0:T(8,128)S(1)}, f32[2,32,2,128]{3,2,1,0:T(2,128)S(1)}, f32[2,2,32]{2,1,0:T(2,128)S(1)}) custom-call(bf16[16,1024]{1,0:T(8,128)(2,1)} %tokens.1, bf16[2,1024,256]{2,1,0:T(8,128)(2,1)} %wq.1, bf16[2,1024,256]{2,1,0:T(8,128)(2,1)} %wk.1, bf16[2,1024,256]{2,1,0:T(8,128)(2,1)} %wv.1, ...), custom_call_target="tpu_custom_call" | custom-call | tf_op jit(solution)/shard_map/pallas_call | solution.py:473
  58.4 3.5 %shard_map.157 = (bf16[16,1024]{1,0:T(8,128)(2,1)}, f32[2,32,2,128,128]{4,3,2,1,0:T(8,128)}, f32[2,32,2,128]{3,2,1,0:T(2,128)}, f32[2,2,32]{2,1,0:T(2,128)}) custom-call(bf16[16,1024]{1,0:T(8,128)(2,1)S(1)} %get-tuple-element.12.rows, f32[2,32,2,128,128]{4,3,2,1,0:T(8,128)S(1)} %get-tuple-element.13.cell, f32[2,32,2,128]{3,2,1,0:T(2,128)S(1)} %get-tuple-element.14.normer, ...), custom_call_target="tpu_custom_call" | custom-call | tf_op jit(solution)/shard_map/pallas_call | solution.py:541

commit v2 on v1

v2 whole, which is shorter than its diff:
```python
import functools
import math

import jax
import jax.numpy as jnp
from jax import lax
from jax.experimental import pallas as pl
from jax.experimental.pallas import tpu as pltpu
from jax.sharding import PartitionSpec as P

EPSILON = 1e-06
F32 = jnp.float32
BF16 = jnp.bfloat16
MESH = pl.DeviceIdType.MESH


def split_axis(size):
    inner = max(f for f in range(1, math.isqrt(size) + 1) if size % f == 0)
    return size // inner, inner


def row_block(index, rows):
    return pl.ds(pl.multiple_of(index * rows, rows), rows)


def gate_dot(scaled, weight):
    return lax.dot_general(
        scaled, weight, (((1,), (1,)), ((), ())), preferred_element_type=F32
    )


def line_order(pos, size):
    low = jnp.minimum(pos, size - 1 - pos)
    order = []
    for k in range(1, size):
        step = (k + 1) // 2
        near = pos + (step if k % 2 == 0 else -step)
        far = jnp.where(2 * pos < size - 1, pos + k - low, pos - k + low)
        order.append(jnp.where(k <= 2 * low, near, far))
    return order


def step_kernel(
    ntp,
    ndp,
    tokens,
    wq,
    wk,
    wv,
    wo,
    wig,
    wfg,
    norm_gain,
    head_gain,
    proj,
    cell,
    normer,
    stab,
    final_out,
    cell_buf,
    normer_out,
    stab_out,
    w_buf,
    ig_buf,
    fg_buf,
    proj_buf,
    written_buf,
    key_buf,
    keep_buf,
    tok_sem,
    small_sem,
    gain_buf,
    head_buf,
    normer_buf,
    stab_buf,
    split_buf,
    current,
    scaled_buf,
    partial,
    gates,
    gate_recv,
    gate_cols,
    pair_recv,
    pair_sum,
    proj_recv,
    gated_all,
    out_part,
    out_stage,
    out_recv,
    load_sem,
    cell_sem,
    ag_send,
    ag_recv,
    pr_send,
    pr_recv,
    rs_send,
    rs_recv,
    gt_send,
    gt_recv,
    gg_send,
    gg_recv,
    os_send,
    os_recv,
):
    blocks = wq.shape[0]
    width, inner = wq.shape[1], wq.shape[2]
    all_heads = wig.shape[1]
    seqs, heads, dh = cell.shape[1], cell.shape[2], cell.shape[3]
    rows = tokens.shape[0]
    batch = rows * ntp
    t = lax.axis_index("tp")
    d = lax.axis_index("dp")
    outer, side = split_axis(ntp)
    z = t // side
    x = lax.rem(t, side)
    z_order = line_order(z, outer)

    pair = 2 if ndp % 2 == 0 else 1
    ring = ndp // pair
    y = d // pair
    core = lax.rem(d, pair)
    own = row_block(d, seqs)
    mine = row_block(t, rows)

    tok_load = pltpu.make_async_copy(tokens, current.at[0, mine], tok_sem)
    tok_load.start()
    barrier = pltpu.get_barrier_semaphore()
    for k in range(1, ntp):
        pl.semaphore_signal(
            barrier, inc=1, device_id={"tp": lax.rem(t + k, ntp)}, device_id_type=MESH
        )
    for k in range(1, ndp):
        pl.semaphore_signal(
            barrier, inc=1, device_id={"dp": lax.rem(d + k, ndp)}, device_id_type=MESH
        )
    small = [
        pltpu.make_async_copy(src, dst, small_sem.at[i])
        for i, (src, dst) in enumerate(
            (
                (norm_gain, gain_buf),
                (head_gain, head_buf),
                (normer, normer_buf),
                (stab, stab_buf),
            )
        )
    ]
    loads = []
    for b in range(blocks):
        one = [
            pltpu.make_async_copy(w.at[b], w_buf.at[b, i], load_sem.at[b, i])
            for i, w in enumerate((wq, wk, wv, wo))
        ]
        one.append(
            pltpu.make_async_copy(
                wig.at[b, :, row_block(d, width)], ig_buf.at[b], load_sem.at[b, 4]
            )
        )
        one.append(
            pltpu.make_async_copy(
                wfg.at[b, :, row_block(d, width)], fg_buf.at[b], load_sem.at[b, 5]
            )
        )
        one.append(pltpu.make_async_copy(proj.at[b], proj_buf.at[b], load_sem.at[b, 6]))
        loads.append(one)
    cell_loads = [
        pltpu.make_async_copy(cell.at[b], cell_buf.at[b], cell_sem.at[b]) for b in range(blocks)
    ]
    tok_load.wait()
    for c in small:
        c.start()
    for b in range(blocks):
        for c in loads[b]:
            c.start()
        cell_loads[b].start()
    pl.semaphore_wait(barrier, ntp - 1 + ndp - 1)

    def split_cells(b):
        cell_loads[b].wait()

        def one(i, _):
            for h in range(heads):
                whole = cell_buf[b, i, h]
                high = whole.astype(BF16)
                here, lanes = row_block(i, dh), slice(h * dh, (h + 1) * dh)
                split_buf[0, here, lanes] = high
                split_buf[1, here, lanes] = (whole - high.astype(F32)).astype(BF16)
            return 0

        lax.fori_loop(0, seqs, one, 0)

    eight = math.gcd(seqs, 8)

    def update_cells(b):
        def one(c, _):
            here = row_block(c, eight)
            keep = keep_buf[here, :]
            for h in range(heads):
                lanes = slice(h * dh, (h + 1) * dh)
                across = jnp.transpose(written_buf[here, lanes])
                keys = key_buf[here, lanes]
                for j in range(eight):
                    cell_buf[b, c * eight + j, h] = (
                        keep[j : j + 1, h : h + 1] * cell_buf[b, c * eight + j, h]
                        + across[:, j : j + 1] * keys[j : j + 1, :]
                    )
            return 0

        lax.fori_loop(0, seqs // eight, one, 0)

    def ag_copy(b, block, slot, dest):
        here = row_block(block, rows)
        return pltpu.make_async_remote_copy(
            src_ref=current.at[b, here],
            dst_ref=current.at[b, here],
            send_sem=ag_send.at[b, slot],
            recv_sem=ag_recv.at[b, slot],
            device_id={"tp": dest},
            device_id_type=MESH,
        )

    def gather_start(b):
        sent = []
        for zd in reversed(z_order):
            sent.append(ag_copy(b, t, lax.rem(zd - z + outer, outer) - 1, zd * side + x))
        for j in range(1, side):
            dest = z * side + lax.rem(x + j, side)
            sent.append(ag_copy(b, t, outer - 1 + (j - 1) * outer, dest))
        for c in sent:
            c.start()
        return sent

    def gather_finish(b, sent):
        for zs in z_order:
            gap = lax.rem(z - zs + outer, outer)
            block = zs * side + x
            ag_copy(b, block, gap - 1, block).wait_recv()
            for j in range(1, side):
                dest = z * side + lax.rem(x + j, side)
                copy = ag_copy(b, block, outer - 1 + (j - 1) * outer + gap, dest)
                copy.start()
                sent.append(copy)
        for j in range(1, side):
            xs = lax.rem(x - j + side, side)
            from_x = z * side + xs
            ag_copy(b, from_x, outer - 1 + (j - 1) * outer, from_x).wait_recv()
            for zs in z_order:
                gap = lax.rem(z - zs + outer, outer)
                slot = outer - 1 + (j - 1) * outer + gap
                ag_copy(b, zs * side + xs, slot, from_x).wait_recv()
        return sent

    gather = gather_start(0)
    for b in range(blocks):
        if b == 0:
            split_cells(0)
            for c in small:
                c.wait()
        sends = gather_finish(b, gather)
        as_float = current[b].astype(F32)
        scaled_buf[...] = (as_float * gain_buf[b : b + 1, :]).astype(BF16)

        def dp_send(src, dst, send_sem, recv_sem, dest):
            copy = pltpu.make_async_remote_copy(
                src_ref=src,
                dst_ref=dst,
                send_sem=send_sem,
                recv_sem=recv_sem,
                device_id={"dp": dest},
                device_id_type=MESH,
            )
            copy.start()
            sends.append(copy)
            return copy

        mate = y * pair + (pair - 1 - core)
        paired = []
        for i in range(4):
            loads[b][i].wait()
            partial[b, i] = jnp.dot(scaled_buf[...], w_buf[b, i], preferred_element_type=F32)
            one = {}
            if pair == 2:
                for k in range(ring):
                    slot = (k + 1) % ring
                    block = row_block(lax.rem(y + slot, ring) * pair + 1 - core, seqs)
                    one[slot] = dp_send(
                        partial.at[b, i, block],
                        pair_recv.at[b, i, slot],
                        pr_send.at[b, i, slot],
                        pr_recv.at[b, i, slot],
                        mate,
                    )
            paired.append(one)

        for c in loads[b][4:]:
            c.wait()
        square = as_float * as_float
        high = square.astype(BF16)
        low = (square - high.astype(F32)).astype(BF16)
        ones = jnp.ones((16, width), BF16)
        squares = gate_dot(ones, high) + gate_dot(ones, low)
        igates = gate_dot(ig_buf[b], scaled_buf[...])
        fgates = gate_dot(fg_buf[b], scaled_buf[...])
        head_row = lax.broadcasted_iota(jnp.int32, (all_heads, batch), 0)
        lines = []
        for source in (igates, fgates):
            for h in range(heads):
                hit = head_row == t * heads + h
                lines.append(jnp.sum(jnp.where(hit, source, 0.0), axis=0, keepdims=True))
        lines.append(squares[0:1])
        line = lax.broadcasted_iota(jnp.int32, gates.shape[1:], 0)
        packed = jnp.zeros(gates.shape[1:], F32)
        for r, value in enumerate(lines):
            packed = jnp.where(line == r, jnp.broadcast_to(value, packed.shape), packed)
        gates[b] = packed
        gate_copies = []
        for k in sorted(range(1, ndp), key=lambda k: -min(k, ndp - k)):
            gate_copies.append(
                dp_send(
                    gates.at[b],
                    gate_recv.at[b, k - 1],
                    gt_send.at[b, k - 1],
                    gt_recv.at[b, k - 1],
                    lax.rem(d + k, ndp),
                )
            )

        arriving = []
        for i in range(4):
            one = []
            for slot in range(1, ring):
                dest = lax.rem(y + slot, ring) * pair + core
                summed = partial[b, i, row_block(dest, seqs), :]
                if pair == 2:
                    paired[i][slot].wait_recv()
                    summed = summed + pair_recv[b, i, slot]
                pair_sum[b, i, slot - 1] = summed
                one.append(
                    dp_send(
                        pair_sum.at[b, i, slot - 1],
                        proj_recv.at[b, i, slot - 1],
                        rs_send.at[b, i, slot - 1],
                        rs_recv.at[b, i, slot - 1],
                        dest,
                    )
                )
            arriving.append(one)

        for c in gate_copies:
            c.wait_recv()
        gate_sum = gates[b]
        for k in range(ndp - 1):
            gate_sum = gate_sum + gate_recv[b, k]
        gate_cols[...] = jnp.transpose(gate_sum)
        pre = gate_cols[own, :]
        inv_rms = lax.rsqrt(pre[:, 2 * heads : 2 * heads + 1] / (width * ndp) + EPSILON)
        pre = pre * inv_rms
        diag = lax.broadcasted_iota(jnp.int32, (seqs, seqs), 0) == (
            lax.broadcasted_iota(jnp.int32, (seqs, seqs), 1)
        )
        lane = lax.broadcasted_iota(jnp.int32, keep_buf.shape, 1)
        aux = jnp.zeros(keep_buf.shape, F32)
        keeps, writes = [], []
        for h in range(heads):
            igate, fpre = pre[:, h : h + 1], pre[:, heads + h : heads + h + 1]
            lf = jnp.minimum(fpre, 0.0) - jnp.log1p(jnp.exp(-jnp.abs(fpre)))
            stab_row = jnp.broadcast_to(stab_buf[b, h : h + 1, :], (seqs, seqs))
            m0 = jnp.sum(jnp.where(diag, stab_row, 0.0), axis=1, keepdims=True)
            carried = lf + m0
            m1 = jnp.maximum(carried, igate)
            stab_out[b, h : h + 1, :] = jnp.sum(jnp.where(diag, m1, 0.0), axis=0, keepdims=True)
            keeps.append(jnp.exp(carried - m1))
            writes.append(jnp.exp(igate - m1))
            aux = jnp.where(lane == h, keeps[h], aux)
        keep_buf[...] = aux

        def total(i):
            value = partial[b, i, own, :]
            if pair == 2:
                paired[i][0].wait_recv()
                value = value + pair_recv[b, i, 0]
            for k in range(ring - 1):
                arriving[i][k].wait_recv()
                value = value + proj_recv[b, i, k]
            return value * inv_rms

        query = total(0)
        wide = -(-2 * heads * seqs // 128) * 128
        column = lax.rem(lax.broadcasted_iota(jnp.int32, (dh, wide), 1), seqs)
        terms = []
        for h in range(heads):
            high = query[:, h * dh : (h + 1) * dh].astype(BF16)
            low = (query[:, h * dh : (h + 1) * dh] - high.astype(F32)).astype(BF16)
            for part in (high, low):
                blank = jnp.zeros(part.shape, BF16)
                terms.append(jnp.concatenate([part if g == h else blank for g in range(heads)], 1))
        if wide > 2 * heads * seqs:
            terms.append(jnp.zeros((wide - 2 * heads * seqs, heads * dh), BF16))
        rhs = jnp.concatenate(terms, 0)
        acc = jnp.zeros((dh, wide), F32)
        for c in range(seqs // eight):
            here = slice(c * eight * dh, (c + 1) * eight * dh)
            prod = gate_dot(split_buf[0, here, :], rhs) + gate_dot(split_buf[1, here, :], rhs)
            for j in range(eight):
                acc = jnp.where(column == c * eight + j, prod[j * dh : (j + 1) * dh], acc)
        turned = jnp.transpose(acc)
        reads = [
            turned[2 * h * seqs : (2 * h + 1) * seqs]
            + turned[(2 * h + 1) * seqs : (2 * h + 2) * seqs]
            for h in range(heads)
        ]
        key = total(1) * (dh ** (-0.5))
        key_buf[...] = key
        dots, normers = [], []
        for h in range(heads):
            lanes = slice(h * dh, (h + 1) * dh)
            qh, kh = query[:, lanes], key[:, lanes]
            n1 = keeps[h] * normer_buf[b, :, h, :] + writes[h] * kh
            normer_out[b, :, h, :] = n1
            dots.append(jnp.sum(kh * qh, axis=1, keepdims=True))
            normers.append(jnp.sum(n1 * qh, axis=1, keepdims=True))
        value = total(2)
        normed = []
        for h in range(heads):
            lanes = slice(h * dh, (h + 1) * dh)
            written = writes[h] * value[:, lanes]
            written_buf[:, lanes] = written
            numer = keeps[h] * reads[h] + written * dots[h]
            readout = numer / jnp.maximum(jnp.abs(normers[h]), 1.0)
            one = readout * lax.rsqrt(jnp.mean(readout * readout, axis=1, keepdims=True) + EPSILON)
            normed.append(one * head_buf[b : b + 1, lanes])
        outgate = total(3)
        for h in range(heads):
            lanes = slice(h * dh, (h + 1) * dh)
            gate = 1.0 / (1.0 + jnp.exp(-outgate[:, lanes]))
            gated_all[b, own, lanes] = (gate * normed[h]).astype(BF16)

        spread = []
        for k in sorted(range(1, ndp), key=lambda k: -min(k, ndp - k)):
            spread.append(
                dp_send(
                    gated_all.at[b, own],
                    gated_all.at[b, own],
                    gg_send.at[b, k - 1],
                    gg_recv.at[b, k - 1],
                    lax.rem(d + k, ndp),
                )
            )
        for c in spread:
            c.wait_recv()
        part = jnp.dot(gated_all[b], proj_buf[b], preferred_element_type=F32)
        out_stage[b] = part.astype(BF16)
        out_part[...] = part
        outs = []
        for zd in list(reversed(z_order)) + [z]:
            for xd in range(1 if zd is z else 0, side):
                dest = zd * side + lax.rem(x + xd, side)
                slot = lax.rem(dest - t + ntp, ntp) - 1
                copy = pltpu.make_async_remote_copy(
                    src_ref=out_stage.at[b, row_block(dest, rows)],
                    dst_ref=out_recv.at[b, slot],
                    send_sem=os_send.at[b, slot],
                    recv_sem=os_recv.at[b, slot],
                    device_id={"tp": dest},
                    device_id_type=MESH,
                )
                copy.start()
                outs.append(copy)
        update_cells(b)
        if b + 1 < blocks:
            split_cells(b + 1)
        for c in outs:
            c.wait_recv()
        summed = out_part[mine, :]
        for k in range(ntp - 1):
            summed = summed + out_recv[b, k].astype(F32)
        if b + 1 < blocks:
            current[b + 1, mine, :] = summed.astype(BF16)
            gather = gather_start(b + 1)
        else:
            final_out[...] = summed.astype(BF16)
        for c in sends + outs:
            c.wait_send()


def store_kernel(rows, cell, normer, stab, rows_out, cell_out, normer_out, stab_out, cell_sem, sems):
    blocks, seqs = cell.shape[0], cell.shape[1]
    parts = cell_sem.shape[1]
    step = seqs // parts
    copies = [
        pltpu.make_async_copy(
            cell.at[b, i * step : (i + 1) * step],
            cell_out.at[b, i * step : (i + 1) * step],
            cell_sem.at[b, i],
        )
        for b in range(blocks)
        for i in range(parts)
    ]
    for i, (src, dst) in enumerate(((rows, rows_out), (normer, normer_out), (stab, stab_out))):
        copies.append(pltpu.make_async_copy(src, dst, sems.at[i]))
    for c in copies:
        c.start()
    for c in copies:
        c.wait()


def per_device(ntp, ndp, *args):
    (tokens, wq, wk, wv, wo, wig, wfg, norm_gain, head_gain, proj, cell, normer, stab) = args
    blocks, width, inner = wq.shape
    all_heads = wig.shape[2]
    seqs, heads, dh = cell.shape[1], cell.shape[2], cell.shape[3]
    rows = tokens.shape[0]
    pair = 2 if ndp % 2 == 0 else 1
    ring = ndp // pair
    more = max(ring - 1, 1)
    wig, wfg, stab = (jnp.swapaxes(a, 1, 2) for a in (wig, wfg, stab))
    batch = rows * ntp
    lanes = -(-heads // 128) * 128
    gate_rows = -(-(2 * heads + 1) // 8) * 8
    vmem = pl.BlockSpec(memory_space=pltpu.VMEM)
    hbm = pl.BlockSpec(memory_space=pltpu.HBM)
    dma = pltpu.SemaphoreType.DMA
    results = pl.pallas_call(
        functools.partial(step_kernel, ntp, ndp),
        out_shape=(
            pltpu.VMEM(tokens.shape, BF16),
            pltpu.VMEM(cell.shape, F32),
            pltpu.VMEM(normer.shape, F32),
            pltpu.VMEM(stab.shape, F32),
        ),
        in_specs=[hbm] * 13,
        out_specs=(vmem,) * 4,
        scratch_shapes=[
            pltpu.VMEM((blocks, 4, width, inner), BF16),
            pltpu.VMEM((blocks, all_heads, width), BF16),
            pltpu.VMEM((blocks, all_heads, width), BF16),
            pltpu.VMEM(proj.shape, BF16),
            pltpu.VMEM((seqs, inner), F32),
            pltpu.VMEM((seqs, inner), F32),
            pltpu.VMEM((seqs, lanes), F32),
            dma,
            dma((4,)),
            pltpu.VMEM(norm_gain.shape, F32),
            pltpu.VMEM(head_gain.shape, F32),
            pltpu.VMEM(normer.shape, F32),
            pltpu.VMEM(stab.shape, F32),
            pltpu.VMEM((2, seqs * dh, heads * dh), BF16),
            pltpu.VMEM((blocks, batch, width), BF16),
            pltpu.VMEM((batch, width), BF16),
            pltpu.VMEM((blocks, 4, batch, inner), F32),
            pltpu.VMEM((blocks, gate_rows, batch), F32),
            pltpu.VMEM((blocks, ndp - 1, gate_rows, batch), F32),
            pltpu.VMEM((batch, gate_rows), F32),
            pltpu.VMEM((blocks, 4, ring, seqs, inner), F32),
            pltpu.VMEM((blocks, 4, more, seqs, inner), F32),
            pltpu.VMEM((blocks, 4, more, seqs, inner), F32),
            pltpu.VMEM((blocks, batch, inner), BF16),
            pltpu.VMEM((batch, width), F32),
            pltpu.VMEM((blocks, batch, width), BF16),
            pltpu.VMEM((blocks, ntp - 1, rows, width), BF16),
            dma((blocks, 7)),
            dma((blocks,)),
            dma((blocks, ntp - 1)),
            dma((blocks, ntp - 1)),
            dma((blocks, 4, ring)),
            dma((blocks, 4, ring)),
            dma((blocks, 4, more)),
            dma((blocks, 4, more)),
            dma((blocks, ndp - 1)),
            dma((blocks, ndp - 1)),
            dma((blocks, ndp - 1)),
            dma((blocks, ndp - 1)),
            dma((blocks, ntp - 1)),
            dma((blocks, ntp - 1)),
        ],
        compiler_params=pltpu.CompilerParams(
            collective_id=0, has_side_effects=True, vmem_limit_bytes=40 << 20
        ),
    )(
        *[
            pltpu.with_memory_space_constraint(a, pltpu.HBM)
            for a in (
                tokens, wq, wk, wv, wo, wig, wfg, norm_gain, head_gain, proj, cell, normer, stab
            )
        ]
    )

    shapes = tuple(jax.ShapeDtypeStruct(a.shape, a.dtype) for a in results)
    rows_out, cell_out, normer_out, stab_out = pl.pallas_call(
        store_kernel,
        out_shape=shapes,
        in_specs=[vmem] * 4,
        out_specs=(hbm,) * 4,
        scratch_shapes=[dma((blocks, math.gcd(seqs, 8))), dma((3,))],
        compiler_params=pltpu.CompilerParams(vmem_limit_bytes=1 << 20),
    )(*results)
    return rows_out, cell_out, normer_out, jnp.swapaxes(stab_out, 1, 2)


def solution(mesh):
    return jax.shard_map(
        functools.partial(per_device, mesh.shape["tp"], mesh.shape["dp"]),
        mesh=mesh,
        in_specs=(
            P("tp", "dp"),
            P(None, "dp", "tp"),
            P(None, "dp", "tp"),
            P(None, "dp", "tp"),
            P(None, "dp", "tp"),
            P(),
            P(),
            P(None, "dp"),
            P(None, "tp"),
            P(None, "tp", "dp"),
            P(None, "dp", "tp", None, None),
            P(None, "dp", "tp", None),
            P(None, "dp", "tp"),
        ),
        out_specs=(
            P("tp", "dp"),
            P(None, "dp", "tp", None, None),
            P(None, "dp", "tp", None),
            P(None, "dp", "tp"),
        ),
        check_vma=False,
    )
```

time: 62 us -> 61.4 us (level)
  Pallas kernels: 61.2 us -> 60.5 us
    pallas_call x1, Pallas kernels: 57.7 us -> 57 us  [per_device(): pl.pallas_call(functools.partial(step_kernel, ntp, ndp), out_shape=(pltpu...]
where the time goes in v2:
time: 61.4 us; the launch traced here: 61.2 us
  Pallas kernels  60.5 us (99%)
  between operations  0.64 us (1%)
    pallas_call x1, Pallas kernels, per_device(): pl.pallas_call(functools.partial(step_kernel, ntp, ndp), out_shape=(pltpu...  57 us
    pallas_call x1, Pallas kernels, per_device(): pl.pallas_call(store_kernel, out_shape=shapes, in_specs=[vmem] * 4, out_s...  3.48 us

profile of v2, /device:TPU:0, one launch (start us, length us, event | category | flops | bytes accessed | tf_op | source)
XLA Modules:
  0.0 61.2 jit_solution(12673915605800434213)
XLA Ops:
  0.6 57.0 %shard_map.156 = (bf16[16,1024]{1,0:T(8,128)(2,1)S(1)}, f32[2,32,2,128,128]{4,3,2,1,0:T(8,128)S(1)}, f32[2,32,2,128]{3,2,1,0:T(2,128)S(1)}, f32[2,2,32]{2,1,0:T(2,128)S(1)}) custom-call(bf16[16,1024]{1,0:T(8,128)(2,1)} %tokens.1, bf16[2,1024,256]{2,1,0:T(8,128)(2,1)} %wq.1, bf16[2,1024,256]{2,1,0:T(8,128)(2,1)} %wk.1, bf16[2,1024,256]{2,1,0:T(8,128)(2,1)} %wv.1, ...), custom_call_target="tpu_custom_call" | custom-call | tf_op jit(solution)/shard_map/pallas_call | solution.py:522
  57.7 3.5 %shard_map.157 = (bf16[16,1024]{1,0:T(8,128)(2,1)}, f32[2,32,2,128,128]{4,3,2,1,0:T(8,128)}, f32[2,32,2,128]{3,2,1,0:T(2,128)}, f32[2,2,32]{2,1,0:T(2,128)}) custom-call(bf16[16,1024]{1,0:T(8,128)(2,1)S(1)} %get-tuple-element.12.rows, f32[2,32,2,128,128]{4,3,2,1,0:T(8,128)S(1)} %get-tuple-element.13.cell, f32[2,32,2,128]{3,2,1,0:T(2,128)S(1)} %get-tuple-element.14.normer, ...), custom_call_target="tpu_custom_call" | custom-call | tf_op jit(solution)/shard_map/pallas_call | solution.py:588

commit v3 on v2

--- a/solution.py
+++ b/solution.py
@@ -168,10 +168,9 @@
     tok_load.wait()
     for c in small:
         c.start()
-    for b in range(blocks):
-        for c in loads[b]:
-            c.start()
-        cell_loads[b].start()
+    for c in loads[0]:
+        c.start()
+    cell_loads[0].start()
     pl.semaphore_wait(barrier, ntp - 1 + ndp - 1)
 
     def split_cells(b):
@@ -251,11 +250,14 @@
 
     gather = gather_start(0)
     for b in range(blocks):
+        sends = gather_finish(b, gather)
         if b == 0:
-            split_cells(0)
             for c in small:
                 c.wait()
-        sends = gather_finish(b, gather)
+            for later in range(1, blocks):
+                for c in loads[later]:
+                    c.start()
+                cell_loads[later].start()
         as_float = current[b].astype(F32)
         scaled_buf[...] = (as_float * gain_buf[b : b + 1, :]).astype(BF16)
 
@@ -273,10 +275,12 @@
             return copy
 
         mate = y * pair + (pair - 1 - core)
+        for i in range(4):
+            loads[b][i].wait()
+        for i in range(4):
+            partial[b, i] = jnp.dot(scaled_buf[...], w_buf[b, i], preferred_element_type=F32)
         paired = []
         for i in range(4):
-            loads[b][i].wait()
-            partial[b, i] = jnp.dot(scaled_buf[...], w_buf[b, i], preferred_element_type=F32)
             one = {}
             if pair == 2:
                 for k in range(ring):
@@ -293,39 +297,43 @@
 
         for c in loads[b][4:]:
             c.wait()
-        square = as_float * as_float
-        high = square.astype(BF16)
-        low = (square - high.astype(F32)).astype(BF16)
-        ones = jnp.ones((16, width), BF16)
-        squares = gate_dot(ones, high) + gate_dot(ones, low)
-        igates = gate_dot(ig_buf[b], scaled_buf[...])
-        fgates = gate_dot(fg_buf[b], scaled_buf[...])
-        head_row = lax.broadcasted_iota(jnp.int32, (all_heads, batch), 0)
-        lines = []
-        for source in (igates, fgates):
-            for h in range(heads):
-                hit = head_row == t * heads + h
-                lines.append(jnp.sum(jnp.where(hit, source, 0.0), axis=0, keepdims=True))
-        lines.append(squares[0:1])
-        line = lax.broadcasted_iota(jnp.int32, gates.shape[1:], 0)
-        packed = jnp.zeros(gates.shape[1:], F32)
-        for r, value in enumerate(lines):
-            packed = jnp.where(line == r, jnp.broadcast_to(value, packed.shape), packed)
-        gates[b] = packed
-        gate_copies = []
-        for k in sorted(range(1, ndp), key=lambda k: -min(k, ndp - k)):
-            gate_copies.append(
-                dp_send(
-                    gates.at[b],
-                    gate_recv.at[b, k - 1],
-                    gt_send.at[b, k - 1],
-                    gt_recv.at[b, k - 1],
-                    lax.rem(d + k, ndp),
-                )
-            )
-
-        arriving = []
-        for i in range(4):
+        gate_copies = [
+            pltpu.make_async_remote_copy(
+                src_ref=gates.at[b],
+                dst_ref=gate_recv.at[b, k - 1],
+                send_sem=gt_send.at[b, k - 1],
+                recv_sem=gt_recv.at[b, k - 1],
+                device_id={"dp": lax.rem(d + k, ndp)},
+                device_id_type=MESH,
+            )
+            for k in sorted(range(1, ndp), key=lambda k: -min(k, ndp - k))
+        ]
+        sends.extend(gate_copies)
+
+        def send_gates():
+            square = current[b].astype(F32) * current[b].astype(F32)
+            high = square.astype(BF16)
+            low = (square - high.astype(F32)).astype(BF16)
+            ones = jnp.ones((16, width), BF16)
+            squares = gate_dot(ones, high) + gate_dot(ones, low)
+            igates = gate_dot(ig_buf[b], scaled_buf[...])
+            fgates = gate_dot(fg_buf[b], scaled_buf[...])
+            head_row = lax.broadcasted_iota(jnp.int32, (all_heads, batch), 0)
+            lines = []
+            for source in (igates, fgates):
+                for h in range(heads):
+                    hit = head_row == t * heads + h
+                    lines.append(jnp.sum(jnp.where(hit, source, 0.0), axis=0, keepdims=True))
+            lines.append(squares[0:1])
+            line = lax.broadcasted_iota(jnp.int32, gates.shape[1:], 0)
+            packed = jnp.zeros(gates.shape[1:], F32)
+            for r, value in enumerate(lines):
+                packed = jnp.where(line == r, jnp.broadcast_to(value, packed.shape), packed)
+            gates[b] = packed
+            for c in gate_copies:
+                c.start()
+
+        def reduce_pair(i):
             one = []
             for slot in range(1, ring):
                 dest = lax.rem(y + slot, ring) * pair + core
@@ -343,8 +351,31 @@
                         dest,
                     )
                 )
-            arriving.append(one)
-
+            return one
+
+        ahead = core == pair - 1 if pair == 2 else d < 0
+        pl.when(ahead)(send_gates)
+        arriving = [reduce_pair(0)]
+        pl.when(jnp.logical_not(ahead))(send_gates)
+        arriving += [reduce_pair(i) for i in range(1, 4)]
+        if b == 0:
+            split_cells(0)
+
+        def total(i):
+            value = partial[b, i, own, :]
+            if pair == 2:
+                value = value + pair_recv[b, i, 0]
+            for k in range(ring - 1):
+                value = value + proj_recv[b, i, k]
+            return value
+
+        def arrived(i):
+            if pair == 2:
+                paired[i][0].wait_recv()
+            for k in range(ring - 1):
+                arriving[i][k].wait_recv()
+
+        arrived(0)
         for c in gate_copies:
             c.wait_recv()
         gate_sum = gates[b]
@@ -373,23 +404,13 @@
             aux = jnp.where(lane == h, keeps[h], aux)
         keep_buf[...] = aux
 
-        def total(i):
-            value = partial[b, i, own, :]
-            if pair == 2:
-                paired[i][0].wait_recv()
-                value = value + pair_recv[b, i, 0]
-            for k in range(ring - 1):
-                arriving[i][k].wait_recv()
-                value = value + proj_recv[b, i, k]
-            return value * inv_rms
-
-        query = total(0)
+        raw = total(0)
         wide = -(-2 * heads * seqs // 128) * 128
         column = lax.rem(lax.broadcasted_iota(jnp.int32, (dh, wide), 1), seqs)
         terms = []
         for h in range(heads):
-            high = query[:, h * dh : (h + 1) * dh].astype(BF16)
-            low = (query[:, h * dh : (h + 1) * dh] - high.astype(F32)).astype(BF16)
+            high = raw[:, h * dh : (h + 1) * dh].astype(BF16)
+            low = (raw[:, h * dh : (h + 1) * dh] - high.astype(F32)).astype(BF16)
             for part in (high, low):
                 blank = jnp.zeros(part.shape, BF16)
                 terms.append(jnp.concatenate([part if g == h else blank for g in range(heads)], 1))
@@ -404,11 +425,17 @@
                 acc = jnp.where(column == c * eight + j, prod[j * dh : (j + 1) * dh], acc)
         turned = jnp.transpose(acc)
         reads = [
-            turned[2 * h * seqs : (2 * h + 1) * seqs]
-            + turned[(2 * h + 1) * seqs : (2 * h + 2) * seqs]
+            (
+                turned[2 * h * seqs : (2 * h + 1) * seqs]
+                + turned[(2 * h + 1) * seqs : (2 * h + 2) * seqs]
+            )
+            * inv_rms
             for h in range(heads)
         ]
-        key = total(1) * (dh ** (-0.5))
+        for i in range(1, 4):
+            arrived(i)
+        query = raw * inv_rms
+        key = total(1) * inv_rms * (dh ** (-0.5))
         key_buf[...] = key
         dots, normers = [], []
         for h in range(heads):
@@ -418,7 +445,7 @@
             normer_out[b, :, h, :] = n1
             dots.append(jnp.sum(kh * qh, axis=1, keepdims=True))
             normers.append(jnp.sum(n1 * qh, axis=1, keepdims=True))
-        value = total(2)
+        value = total(2) * inv_rms
         normed = []
         for h in range(heads):
             lanes = slice(h * dh, (h + 1) * dh)
@@ -428,7 +455,7 @@
             readout = numer / jnp.maximum(jnp.abs(normers[h]), 1.0)
             one = readout * lax.rsqrt(jnp.mean(readout * readout, axis=1, keepdims=True) + EPSILON)
             normed.append(one * head_buf[b : b + 1, lanes])
-        outgate = total(3)
+        outgate = total(3) * inv_rms
         for h in range(heads):
             lanes = slice(h * dh, (h + 1) * dh)
             gate = 1.0 / (1.0 + jnp.exp(-outgate[:, lanes]))

time: 61.4 us -> 60 us (0.977)
  Pallas kernels: 60.5 us -> 59.2 us
    pallas_call x1, Pallas kernels: 57 us -> 55.7 us  [per_device(): pl.pallas_call(functools.partial(step_kernel, ntp, ndp), out_shape=(pltpu...]
where the time goes in v3:
time: 60 us; the launch traced here: 59.8 us
  Pallas kernels  59.2 us (99%)
  between operations  0.64 us (1%)
    pallas_call x1, Pallas kernels, per_device(): pl.pallas_call(functools.partial(step_kernel, ntp, ndp), out_shape=(pltpu...  55.7 us
    pallas_call x1, Pallas kernels, per_device(): pl.pallas_call(store_kernel, out_shape=shapes, in_specs=[vmem] * 4, out_s...  3.48 us

profile of v3, /device:TPU:0, one launch (start us, length us, event | category | flops | bytes accessed | tf_op | source)
XLA Modules:
  0.0 59.8 jit_solution(18388465475094322296)
XLA Ops:
  0.6 55.7 %shard_map.156 = (bf16[16,1024]{1,0:T(8,128)(2,1)S(1)}, f32[2,32,2,128,128]{4,3,2,1,0:T(8,128)S(1)}, f32[2,32,2,128]{3,2,1,0:T(2,128)S(1)}, f32[2,2,32]{2,1,0:T(2,128)S(1)}) custom-call(bf16[16,1024]{1,0:T(8,128)(2,1)} %tokens.1, bf16[2,1024,256]{2,1,0:T(8,128)(2,1)} %wq.1, bf16[2,1024,256]{2,1,0:T(8,128)(2,1)} %wk.1, bf16[2,1024,256]{2,1,0:T(8,128)(2,1)} %wv.1, ...), custom_call_target="tpu_custom_call" | custom-call | tf_op jit(solution)/shard_map/pallas_call | solution.py:549
  56.4 3.5 %shard_map.157 = (bf16[16,1024]{1,0:T(8,128)(2,1)}, f32[2,32,2,128,128]{4,3,2,1,0:T(8,128)}, f32[2,32,2,128]{3,2,1,0:T(2,128)}, f32[2,2,32]{2,1,0:T(2,128)}) custom-call(bf16[16,1024]{1,0:T(8,128)(2,1)S(1)} %get-tuple-element.12.rows, f32[2,32,2,128,128]{4,3,2,1,0:T(8,128)S(1)} %get-tuple-element.13.cell, f32[2,32,2,128]{3,2,1,0:T(2,128)S(1)} %get-tuple-element.14.normer, ...), custom_call_target="tpu_custom_call" | custom-call | tf_op jit(solution)/shard_map/pallas_call | solution.py:615

commit v4 on v3

--- a/solution.py
+++ b/solution.py
@@ -75,18 +75,24 @@
     stab_buf,
     split_buf,
     current,
+    mixed,
     scaled_buf,
     partial,
+    mixed_partial,
     gates,
     gate_recv,
     gate_cols,
     pair_recv,
     pair_sum,
     proj_recv,
+    pair_narrow,
+    narrow_recv,
     gated_all,
     out_part,
     out_stage,
     out_recv,
+    mix_stage,
+    mix_recv,
     load_sem,
     cell_sem,
     ag_send,
@@ -101,6 +107,8 @@
     gg_recv,
     os_send,
     os_recv,
+    ms_send,
+    ms_recv,
 ):
     blocks = wq.shape[0]
     width, inner = wq.shape[1], wq.shape[2]
@@ -121,8 +129,9 @@
     core = lax.rem(d, pair)
     own = row_block(d, seqs)
     mine = row_block(t, rows)
-
-    tok_load = pltpu.make_async_copy(tokens, current.at[0, mine], tok_sem)
+    few, half = seqs // outer, width // side
+
+    tok_load = pltpu.make_async_copy(tokens, current.at[mine], tok_sem)
     tok_load.start()
     barrier = pltpu.get_barrier_semaphore()
     for k in range(1, ntp):
@@ -182,7 +191,8 @@
                 high = whole.astype(BF16)
                 here, lanes = row_block(i, dh), slice(h * dh, (h + 1) * dh)
                 split_buf[0, here, lanes] = high
-                split_buf[1, here, lanes] = (whole - high.astype(F32)).astype(BF16)
+                if b + 1 < blocks:
+                    split_buf[1, here, lanes] = (whole - high.astype(F32)).astype(BF16)
             return 0
 
         lax.fori_loop(0, seqs, one, 0)
@@ -207,10 +217,13 @@
         lax.fori_loop(0, seqs // eight, one, 0)
 
     def ag_copy(b, block, slot, dest):
-        here = row_block(block, rows)
+        if b == 0:
+            here = current.at[row_block(block, rows)]
+        else:
+            here = mixed.at[b - 1, lax.rem(block, side), block // side]
         return pltpu.make_async_remote_copy(
-            src_ref=current.at[b, here],
-            dst_ref=current.at[b, here],
+            src_ref=here,
+            dst_ref=here,
             send_sem=ag_send.at[b, slot],
             recv_sem=ag_recv.at[b, slot],
             device_id={"tp": dest},
@@ -258,8 +271,19 @@
                 for c in loads[later]:
                     c.start()
                 cell_loads[later].start()
-        as_float = current[b].astype(F32)
-        scaled_buf[...] = (as_float * gain_buf[b : b + 1, :]).astype(BF16)
+        def load_current():
+            if b == 0:
+                return current[...].astype(F32)
+            parts = [mixed[b - 1, i].reshape(batch, half).astype(F32) for i in range(side)]
+            return jnp.concatenate(parts, 1)
+
+        def seq_rows(i, block):
+            return partial.at[i, block] if b == 0 else mixed_partial.at[b - 1, i, :, block]
+
+        def narrow(i):
+            return b + 1 == blocks and i >= 2
+
+        scaled_buf[...] = (load_current() * gain_buf[b : b + 1, :]).astype(BF16)
 
         def dp_send(src, dst, send_sem, recv_sem, dest):
             copy = pltpu.make_async_remote_copy(
@@ -278,16 +302,20 @@
         for i in range(4):
             loads[b][i].wait()
         for i in range(4):
-            partial[b, i] = jnp.dot(scaled_buf[...], w_buf[b, i], preferred_element_type=F32)
+            product = jnp.dot(scaled_buf[...], w_buf[b, i], preferred_element_type=F32)
+            if b == 0:
+                partial[i] = product.reshape(ndp, outer, few, inner)
+            else:
+                mixed_partial[b - 1, i] = product.reshape(outer, ndp, few, inner)
         paired = []
         for i in range(4):
             one = {}
             if pair == 2:
                 for k in range(ring):
                     slot = (k + 1) % ring
-                    block = row_block(lax.rem(y + slot, ring) * pair + 1 - core, seqs)
+                    block = lax.rem(y + slot, ring) * pair + 1 - core
                     one[slot] = dp_send(
-                        partial.at[b, i, block],
+                        seq_rows(i, block),
                         pair_recv.at[b, i, slot],
                         pr_send.at[b, i, slot],
                         pr_recv.at[b, i, slot],
@@ -311,7 +339,8 @@
         sends.extend(gate_copies)
 
         def send_gates():
-            square = current[b].astype(F32) * current[b].astype(F32)
+            plain = load_current()
+            square = plain * plain
             high = square.astype(BF16)
             low = (square - high.astype(F32)).astype(BF16)
             ones = jnp.ones((16, width), BF16)
@@ -337,15 +366,19 @@
             one = []
             for slot in range(1, ring):
                 dest = lax.rem(y + slot, ring) * pair + core
-                summed = partial[b, i, row_block(dest, seqs), :]
+                summed = seq_rows(i, dest)[...]
                 if pair == 2:
                     paired[i][slot].wait_recv()
                     summed = summed + pair_recv[b, i, slot]
-                pair_sum[b, i, slot - 1] = summed
+                if narrow(i):
+                    src, dst = pair_narrow.at[i - 2, slot - 1], narrow_recv.at[i - 2, slot - 1]
+                else:
+                    src, dst = pair_sum.at[b, i, slot - 1], proj_recv.at[b, i, slot - 1]
+                src[...] = summed.astype(src.dtype).reshape(src.shape)
                 one.append(
                     dp_send(
-                        pair_sum.at[b, i, slot - 1],
-                        proj_recv.at[b, i, slot - 1],
+                        src,
+                        dst,
                         rs_send.at[b, i, slot - 1],
                         rs_recv.at[b, i, slot - 1],
                         dest,
@@ -362,11 +395,15 @@
             split_cells(0)
 
         def total(i):
-            value = partial[b, i, own, :]
+            value = seq_rows(i, d)[...]
             if pair == 2:
                 value = value + pair_recv[b, i, 0]
+            value = value.reshape(seqs, inner)
             for k in range(ring - 1):
-                value = value + proj_recv[b, i, k]
+                if narrow(i):
+                    value = value + narrow_recv[i - 2, k].astype(F32)
+                else:
+                    value = value + proj_recv[b, i, k].reshape(seqs, inner)
             return value
 
         def arrived(i):
@@ -382,7 +419,12 @@
         for k in range(ndp - 1):
             gate_sum = gate_sum + gate_recv[b, k]
         gate_cols[...] = jnp.transpose(gate_sum)
-        pre = gate_cols[own, :]
+        if b == 0:
+            pre = gate_cols[own, :]
+        else:
+            pre = jnp.concatenate(
+                [gate_cols[row_block(i * ndp + d, few), :] for i in range(outer)], 0
+            )
         inv_rms = lax.rsqrt(pre[:, 2 * heads : 2 * heads + 1] / (width * ndp) + EPSILON)
         pre = pre * inv_rms
         diag = lax.broadcasted_iota(jnp.int32, (seqs, seqs), 0) == (
@@ -420,7 +462,9 @@
         acc = jnp.zeros((dh, wide), F32)
         for c in range(seqs // eight):
             here = slice(c * eight * dh, (c + 1) * eight * dh)
-            prod = gate_dot(split_buf[0, here, :], rhs) + gate_dot(split_buf[1, here, :], rhs)
+            prod = gate_dot(split_buf[0, here, :], rhs)
+            if b + 1 < blocks:
+                prod = prod + gate_dot(split_buf[1, here, :], rhs)
             for j in range(eight):
                 acc = jnp.where(column == c * eight + j, prod[j * dh : (j + 1) * dh], acc)
         turned = jnp.transpose(acc)
@@ -461,32 +505,78 @@
             gate = 1.0 / (1.0 + jnp.exp(-outgate[:, lanes]))
             gated_all[b, own, lanes] = (gate * normed[h]).astype(BF16)
 
-        spread = []
-        for k in sorted(range(1, ndp), key=lambda k: -min(k, ndp - k)):
-            spread.append(
-                dp_send(
-                    gated_all.at[b, own],
-                    gated_all.at[b, own],
-                    gg_send.at[b, k - 1],
-                    gg_recv.at[b, k - 1],
-                    lax.rem(d + k, ndp),
-                )
-            )
-        for c in spread:
-            c.wait_recv()
-        part = jnp.dot(gated_all[b], proj_buf[b], preferred_element_type=F32)
-        out_stage[b] = part.astype(BF16)
-        out_part[...] = part
+        spread = {}
+        reach = sorted(range(1, ndp), key=lambda k: -min(k, ndp - k))
+        for k in reach:
+            spread[k] = dp_send(
+                gated_all.at[b, own],
+                gated_all.at[b, own],
+                gg_send.at[b, k - 1],
+                gg_recv.at[b, k - 1],
+                lax.rem(d + k, ndp),
+            )
         outs = []
-        for zd in list(reversed(z_order)) + [z]:
-            for xd in range(1 if zd is z else 0, side):
-                dest = zd * side + lax.rem(x + xd, side)
+        targets = [
+            (zd, lax.rem(x + i, side))
+            for zd in list(reversed(z_order)) + [z]
+            for i in range(1 if zd is z else 0, side)
+        ]
+        if b + 1 < blocks:
+            def multiply(peer):
+                block = row_block(peer, seqs)
+                part = jnp.dot(gated_all[b, block, :], proj_buf[b], preferred_element_type=F32)
+                out_part[block, :] = part
+                for i in range(side):
+                    piece = part[:, i * half : (i + 1) * half].astype(BF16)
+                    mix_stage[b, i, :, peer] = piece.reshape(outer, few, half)
+                for zd, xd in targets:
+                    slot = lax.rem(zd * side + xd - t + ntp, ntp) - 1
+                    copy = pltpu.make_async_remote_copy(
+                        src_ref=mix_stage.at[b, xd, zd, peer],
+                        dst_ref=mix_recv.at[b, slot, peer],
+                        send_sem=ms_send.at[b, slot, peer],
+                        recv_sem=ms_recv.at[b, slot, peer],
+                        device_id={"tp": zd * side + xd},
+                        device_id_type=MESH,
+                    )
+                    copy.start()
+                    outs.append(copy)
+
+            def landed(gap):
+                src = lax.rem(d + ndp - gap, ndp)
+                pltpu.make_async_remote_copy(
+                    src_ref=gated_all.at[b, own],
+                    dst_ref=gated_all.at[b, row_block(src, seqs)],
+                    send_sem=gg_send.at[b, gap - 1],
+                    recv_sem=gg_recv.at[b, gap - 1],
+                    device_id={"dp": src},
+                    device_id_type=MESH,
+                ).wait_recv()
+
+            multiply(d)
+            if pair == 2:
+                landed(lax.rem(d - mate + ndp, ndp))
+                multiply(mate)
+            for step in range(1, ring):
+                yp = lax.rem(y + step, ring)
+                for i in range(pair):
+                    peer = yp * pair + lax.rem(core + i, pair)
+                    landed(lax.rem(d - peer + ndp, ndp))
+                    multiply(peer)
+        else:
+            for c in spread.values():
+                c.wait_recv()
+            part = jnp.dot(gated_all[b], proj_buf[b], preferred_element_type=F32)
+            out_stage[...] = part.astype(BF16)
+            out_part[...] = part
+            for zd, xd in targets:
+                dest = zd * side + xd
                 slot = lax.rem(dest - t + ntp, ntp) - 1
                 copy = pltpu.make_async_remote_copy(
-                    src_ref=out_stage.at[b, row_block(dest, rows)],
-                    dst_ref=out_recv.at[b, slot],
-                    send_sem=os_send.at[b, slot],
-                    recv_sem=os_recv.at[b, slot],
+                    src_ref=out_stage.at[row_block(dest, rows)],
+                    dst_ref=out_recv.at[slot],
+                    send_sem=os_send.at[slot],
+                    recv_sem=os_recv.at[slot],
                     device_id={"tp": dest},
                     device_id_type=MESH,
                 )
@@ -497,13 +587,18 @@
             split_cells(b + 1)
         for c in outs:
             c.wait_recv()
-        summed = out_part[mine, :]
-        for k in range(ntp - 1):
-            summed = summed + out_recv[b, k].astype(F32)
         if b + 1 < blocks:
-            current[b + 1, mine, :] = summed.astype(BF16)
+            columns = pl.ds(pl.multiple_of(x * half, half), half)
+            for peer in range(ndp):
+                summed = out_part[row_block(peer * outer + z, few), columns]
+                for k in range(ntp - 1):
+                    summed = summed + mix_recv[b, k, peer].astype(F32)
+                mixed[b, x, z, peer] = summed.astype(BF16)
             gather = gather_start(b + 1)
         else:
+            summed = out_part[mine, :]
+            for k in range(ntp - 1):
+                summed = summed + out_recv[k].astype(F32)
             final_out[...] = summed.astype(BF16)
         for c in sends + outs:
             c.wait_send()
@@ -539,6 +634,9 @@
     pair = 2 if ndp % 2 == 0 else 1
     ring = ndp // pair
     more = max(ring - 1, 1)
+    passed = max(blocks - 1, 1)
+    outer, side = split_axis(ntp)
+    few = seqs // outer
     wig, wfg, stab = (jnp.swapaxes(a, 1, 2) for a in (wig, wfg, stab))
     batch = rows * ntp
     lanes = -(-heads // 128) * 128
@@ -571,19 +669,25 @@
             pltpu.VMEM(normer.shape, F32),
             pltpu.VMEM(stab.shape, F32),
             pltpu.VMEM((2, seqs * dh, heads * dh), BF16),
-            pltpu.VMEM((blocks, batch, width), BF16),
             pltpu.VMEM((batch, width), BF16),
-            pltpu.VMEM((blocks, 4, batch, inner), F32),
+            pltpu.VMEM((passed, side, outer, ndp, few, width // side), BF16),
+            pltpu.VMEM((batch, width), BF16),
+            pltpu.VMEM((4, ndp, outer, few, inner), F32),
+            pltpu.VMEM((passed, 4, outer, ndp, few, inner), F32),
             pltpu.VMEM((blocks, gate_rows, batch), F32),
             pltpu.VMEM((blocks, ndp - 1, gate_rows, batch), F32),
             pltpu.VMEM((batch, gate_rows), F32),
-            pltpu.VMEM((blocks, 4, ring, seqs, inner), F32),
-            pltpu.VMEM((blocks, 4, more, seqs, inner), F32),
-            pltpu.VMEM((blocks, 4, more, seqs, inner), F32),
+            pltpu.VMEM((blocks, 4, ring, outer, few, inner), F32),
+            pltpu.VMEM((blocks, 4, more, outer, few, inner), F32),
+            pltpu.VMEM((blocks, 4, more, outer, few, inner), F32),
+            pltpu.VMEM((2, more, seqs, inner), BF16),
+            pltpu.VMEM((2, more, seqs, inner), BF16),
             pltpu.VMEM((blocks, batch, inner), BF16),
             pltpu.VMEM((batch, width), F32),
-            pltpu.VMEM((blocks, batch, width), BF16),
-            pltpu.VMEM((blocks, ntp - 1, rows, width), BF16),
+            pltpu.VMEM((batch, width), BF16),
+            pltpu.VMEM((ntp - 1, rows, width), BF16),
+            pltpu.VMEM((passed, side, outer, ndp, few, width // side), BF16),
+            pltpu.VMEM((passed, ntp - 1, ndp, few, width // side), BF16),
             dma((blocks, 7)),
             dma((blocks,)),
             dma((blocks, ntp - 1)),
@@ -596,8 +700,10 @@
             dma((blocks, ndp - 1)),
             dma((blocks, ndp - 1)),
             dma((blocks, ndp - 1)),
-            dma((blocks, ntp - 1)),
-            dma((blocks, ntp - 1)),
+            dma((ntp - 1,)),
+            dma((ntp - 1,)),
+            dma((passed, ntp - 1, ndp)),
+            dma((passed, ntp - 1, ndp)),
         ],
         compiler_params=pltpu.CompilerParams(
             collective_id=0, has_side_effects=True, vmem_limit_bytes=40 << 20

time: 60 us -> 57.1 us (0.952)
  Pallas kernels: 59.2 us -> 56.2 us
    pallas_call x1, Pallas kernels: 55.7 us -> 52.8 us  [per_device(): pl.pallas_call(functools.partial(step_kernel, ntp, ndp), out_shape=(pltpu...]
where the time goes in v4:
time: 57.1 us; the launch traced here: 56.9 us
  Pallas kernels  56.2 us (98%)
  between operations  0.64 us (1%)
    pallas_call x1, Pallas kernels, per_device(): pl.pallas_call(functools.partial(step_kernel, ntp, ndp), out_shape=(pltpu...  52.8 us
    pallas_call x1, Pallas kernels, per_device(): pl.pallas_call(store_kernel, out_shape=shapes, in_specs=[vmem] * 4, out_s...  3.48 us

profile of v4, /device:TPU:0, one launch (start us, length us, event | category | flops | bytes accessed | tf_op | source)
XLA Modules:
  0.0 56.9 jit_solution(14489583309025272394)
XLA Ops:
  0.6 52.8 %shard_map.156 = (bf16[16,1024]{1,0:T(8,128)(2,1)S(1)}, f32[2,32,2,128,128]{4,3,2,1,0:T(8,128)S(1)}, f32[2,32,2,128]{3,2,1,0:T(2,128)S(1)}, f32[2,2,32]{2,1,0:T(2,128)S(1)}) custom-call(bf16[16,1024]{1,0:T(8,128)(2,1)} %tokens.1, bf16[2,1024,256]{2,1,0:T(8,128)(2,1)} %wq.1, bf16[2,1024,256]{2,1,0:T(8,128)(2,1)} %wk.1, bf16[2,1024,256]{2,1,0:T(8,128)(2,1)} %wv.1, ...), custom_call_target="tpu_custom_call" | custom-call | tf_op jit(solution)/shard_map/pallas_call | solution.py:647
  53.4 3.5 %shard_map.157 = (bf16[16,1024]{1,0:T(8,128)(2,1)}, f32[2,32,2,128,128]{4,3,2,1,0:T(8,128)}, f32[2,32,2,128]{3,2,1,0:T(2,128)}, f32[2,2,32]{2,1,0:T(2,128)}) custom-call(bf16[16,1024]{1,0:T(8,128)(2,1)S(1)} %get-tuple-element.12.rows, f32[2,32,2,128,128]{4,3,2,1,0:T(8,128)S(1)} %get-tuple-element.13.cell, f32[2,32,2,128]{3,2,1,0:T(2,128)S(1)} %get-tuple-element.14.normer, ...), custom_call_target="tpu_custom_call" | custom-call | tf_op jit(solution)/shard_map/pallas_call | solution.py:721
